TPU v7x, 128 devices: a whole 4x4x4 slice. The times are simulated.
128 devices in a mesh: gr: 2 (over z_hi), fs: 32 (over z_lo, y, x), tp: 2 (over core).
Axes of the slice: x: 4, y: 4, z: 4 (z_hi: 2, z_lo: 2; z = z_hi * 2 + z_lo), core: 2. Of those that a mesh axis runs over, the one named last changes fastest.
Arguments:
- tokens: bfloat16 [4, 2048, 2048], P(('gr', 'tp')), may hold values from -6 to 6
- gate_master: float32 [3, 2048, 7168], P(None, 'fs', ('gr', 'tp')), may hold values from -0.125 to 0.125
- up_master: float32 [3, 2048, 7168], P(None, 'fs', ('gr', 'tp')), may hold values from -0.125 to 0.125
- down_master: float32 [3, 7168, 2048], P(None, 'fs', ('gr', 'tp')), may hold values from -0.0625 to 0.0625
- norm_gain: float32 [2048], P('fs'), may hold values from 0.1 to 1.9
- route: int32 [4, 2048, 2], P(('gr', 'tp')), may hold values from 0 to 2, all different within a row
- route_weight: float32 [4, 2048, 2], P(('gr', 'tp')), may hold values from 0.05 to 1
Outputs:
- gate_out: bfloat16 [3, 2048, 7168], P(None, None, 'fs')
- up_out: bfloat16 [3, 2048, 7168], P(None, None, 'fs')
- down_out: bfloat16 [3, 7168, 2048], P(None, 'fs')
- mixed: bfloat16 [4, 2048, 2048], P(('gr', 'tp'), 'fs')
Inputs may be any that keep to these rules, and one draw needn't show every extreme that they name: `route`: each token names two different experts; every expert is named by some token.
All inputs are finite; a program needn't handle non-finite values.
Results may differ from a plain program's by a relative error of at most 0.024.
Values may be sent and summed in bfloat16 or wider, within the bound.
No kernel may reach another device: no remote copies, remote signals or barrier semaphores. Data moves between devices by JAX's collectives and lax.ppermute only.
A program may use at most 192 MiB of HBM per device.

v0:
```python
import jax
import jax.numpy as jnp
from jax import lax
from jax.sharding import Mesh
from jax.sharding import PartitionSpec as P

FS = ("fs_0", "fs_1", "fs_2")


def reduced_to_own(blocks, axes, order):
    dims = [lax.axis_size(a) for a in axes]
    blocks = blocks.reshape(*dims, *blocks.shape[1:])
    blocks = blocks.transpose(*order, *range(len(axes), blocks.ndim))
    blocks = blocks.reshape(-1, *blocks.shape[len(axes) :])
    for k in order:
        blocks = lax.psum_scatter(blocks, axes[k], scatter_dimension=0, tiled=True)
    return blocks[0]


def split_up(array, dim, peers):
    dims = array.shape
    blocks = array.reshape(*dims[:dim], peers, dims[dim] // peers, *dims[dim + 1 :])
    return jnp.moveaxis(blocks, dim, 0)


def sum_by_axis_2(array, axes, order, dim):
    peers = lax.axis_size(axes)
    return reduced_to_own(split_up(array, dim, peers), axes, order)


def normalize(rows_in):
    values = rows_in.astype(jnp.float32)
    scaled = values * lax.rsqrt(jnp.mean(values * values, axis=-1, keepdims=True) + 1e-06)
    return scaled.astype(jnp.bfloat16)


def mixing(chosen, weights, experts):
    share = weights / jnp.sum(weights, axis=-1, keepdims=True)
    labels = jnp.arange(experts, dtype=jnp.int32)
    match = (chosen[:, :, None] == labels[None, None, :]).astype(jnp.float32)
    return jnp.sum(share[:, :, None] * match, axis=1)


def expert_term(normed, mix_column, gate_weight, up_weight, down_weight):
    gate_act = jnp.dot(normed, gate_weight, preferred_element_type=jnp.float32)
    up_act = jnp.dot(normed, up_weight, preferred_element_type=jnp.float32)
    hidden = (jax.nn.silu(gate_act) * up_act).astype(jnp.bfloat16)
    projected = jnp.dot(hidden, down_weight, preferred_element_type=jnp.float32)
    return mix_column * projected


def shards(tokens, gate_master, up_master, down_master, norm_gain, route, route_weight):
    scaled_gain = norm_gain[None, :, None]
    gate_local = (scaled_gain * gate_master).astype(jnp.bfloat16)
    up_local = (scaled_gain * up_master).astype(jnp.bfloat16)
    down_local = down_master.astype(jnp.bfloat16)
    experts = gate_local.shape[0]
    normed = normalize(tokens[0])
    combine = mixing(route[0], route_weight[0], experts)
    width = normed.shape[1]
    gate_rows, up_rows, down_out = (
        lax.all_gather(gate_local, ("gr", "tp"), axis=2, tiled=True),
        lax.all_gather(up_local, ("gr", "tp"), axis=2, tiled=True),
        lax.all_gather(down_local, ("gr", "tp"), axis=2, tiled=True),
    )
    gate_out, up_out = (
        lax.all_to_all(gate_rows, FS, split_axis=2, concat_axis=1, tiled=True),
        lax.all_to_all(up_rows, FS, split_axis=2, concat_axis=1, tiled=True),
    )
    own_rows = normed.shape[0] // lax.axis_size(FS)
    total = jnp.zeros((own_rows * lax.axis_size(FS), width), jnp.float32)
    for index in range(experts):
        total = total + expert_term(
            normed, combine[:, index : index + 1], gate_out[index], up_out[index], down_out[index]
        )
    summed = sum_by_axis_2(total.astype(jnp.bfloat16), FS, (1, 2, 0), 0).astype(jnp.float32)
    mixed = summed.astype(jnp.bfloat16)[None]
    return (gate_out, up_out, down_out, mixed)


def solution(mesh):
    split = Mesh(
        mesh.devices.reshape(mesh.shape["gr"], 2, 4, 4, mesh.shape["tp"]),
        ("gr", "fs_0", "fs_1", "fs_2", "tp"),
    )
    in_specs = (
        P(("gr", "tp"), None, None),
        P(None, FS, ("gr", "tp")),
        P(None, FS, ("gr", "tp")),
        P(None, FS, ("gr", "tp")),
        P(FS),
        P(("gr", "tp"), None, None),
        P(("gr", "tp"), None, None),
    )
    out_specs = (P(None, None, FS), P(None, None, FS), P(None, FS, None), P(("gr", "tp"), FS, None))
    return jax.shard_map(
        shards, mesh=split, in_specs=in_specs, out_specs=out_specs, check_vma=False
    )
```

profile of v0, /device:TPU:1, one launch (start us, length us, event | category | flops | bytes accessed | tf_op | source)
XLA Modules:
  0.0 390.9 jit_solution(5299467397481243480)
XLA Ops:
  7.2 3.1 multiply_convert_fusion
  11.1 33.5 %all-gather.4.cloned.1.call-done = bf16[3,64,7168]{2,1,0:T(8,128)(2,1)} async-done(((bf16[3,64,1792]{2,1,0:T(8,128)(2,1)}), bf16[3,64,7168]{2,1,0:T(8,128)(2,1)}) %all-gather.4.cloned.1.call-update) | async-done | bytes 2752528 | tf_op jit(solution)/shard_map/all_gather | solution.py:62
  44.5 10.1 %copy.41 = bf16[3,64,7168]{1,0,2:T(4,128)(2,1)} copy(bf16[3,64,7168]{2,1,0:T(8,128)(2,1)} %all-gather.4.cloned.1.call-done) | data formatting | bytes 5505024 | tf_op jit(solution)/shard_map/all_gather | solution.py:62
  54.6 12.6 %reshape.105 = bf16[32,2,21504]{2,1,0:T(2,128)(2,1)} reshape(bf16[7168,3,64]{2,1,0:T(4,128)(2,1)} %bitcast.55) | data formatting | bytes 5505024
  67.2 7.0 %all-to-all-start = ((bf16[32,2,21504]{2,1,0:T(2,128)(2,1)}), bf16[32,2,21504]{2,1,0:T(2,128)(2,1)S(1)}, u32[]{:S(2)}, u32[]{:S(2)}) async-start(bf16[32,2,21504]{2,1,0:T(2,128)(2,1)} %reshape.105), calls=%async_computation | async-start | bytes 5505024 | tf_op jit(solution)/shard_map/all_to_all | solution.py:67
  74.3 2.3 convert_element_type.47
  76.7 10.1 %copy.43 = bf16[3,64,7168]{1,0,2:T(4,128)(2,1)} copy(bf16[3,64,7168]{2,1,0:T(8,128)(2,1)} %all-gather.6.cloned.1.call-done) | data formatting | bytes 5505024 | tf_op jit(solution)/shard_map/all_gather | solution.py:63
  86.8 12.6 %reshape.107 = bf16[32,2,21504]{2,1,0:T(2,128)(2,1)} reshape(bf16[7168,3,64]{2,1,0:T(4,128)(2,1)} %bitcast.56) | data formatting | bytes 5505024
  99.4 9.2 %all-to-all-done = bf16[32,2,21504]{2,1,0:T(2,128)(2,1)S(1)} async-done(((bf16[32,2,21504]{2,1,0:T(2,128)(2,1)}), bf16[32,2,21504]{2,1,0:T(2,128)(2,1)S(1)}, u32[]{:S(2)}, u32[]{:S(2)}) %all-to-all-start) | async-done | bytes 2752544 | tf_op jit(solution)/shard_map/all_to_all | solution.py:67
  108.6 6.3 %all-to-all-start.1 = ((bf16[32,2,21504]{2,1,0:T(2,128)(2,1)}), bf16[32,2,21504]{2,1,0:T(2,128)(2,1)}, u32[]{:S(2)}, u32[]{:S(2)}) async-start(bf16[32,2,21504]{2,1,0:T(2,128)(2,1)} %reshape.107), calls=%async_computation.1 | async-start | bytes 5505024 | tf_op jit(solution)/shard_map/all_to_all | solution.py:68
  115.1 5.1 %fusion = f32[2048]{0:T(1024)S(1)} fusion(bf16[1,2048,2048]{2,1,0:T(8,128)(2,1)} %param.7), kind=kLoop, calls=%fused_computation.2 | loop fusion | flops 12580864 | bytes 8396800 | tf_op jit(solution)/shard_map/reduce_sum | solution.py:33
  120.3 8.0 %fusion.2 = bf16[2048,2048]{1,0:T(8,128)(2,1)} fusion(bf16[1,2048,2048]{2,1,0:T(8,128)(2,1)} %param.7, f32[2048]{0:T(1024)S(1)} %add_rsqrt_fusion), kind=kLoop, calls=%fused_computation.5 | loop fusion | flops 12582912 | bytes 16785408 | tf_op jit(solution)/shard_map/convert_element_type | solution.py:34
  128.3 8.7 %reshape.106 = bf16[7168,3,64]{2,1,0:T(4,128)(2,1)} reshape(bf16[32,2,21504]{2,1,0:T(2,128)(2,1)S(1)} %all-to-all-done) | data formatting | bytes 5505024
  136.9 10.7 %copy.42 = bf16[3,64,32,224]{3,1,2,0:T(8,128)(2,1)S(1)} copy(bf16[3,64,32,224]{1,0,3,2:T(4,128)(2,1)} %bitcast.57) | data formatting | bytes 5505024 | tf_op jit(solution)/shard_map/all_to_all | solution.py:67
  147.7 0.9 all-to-all-done.1
  148.6 12.5 %reshape.108 = bf16[7168,3,64]{2,1,0:T(4,128)(2,1)} reshape(bf16[32,2,21504]{2,1,0:T(2,128)(2,1)} %all-to-all-done.1) | data formatting | bytes 5505024
  161.0 11.4 %copy.44 = bf16[3,64,32,224]{3,1,2,0:T(8,128)(2,1)} copy(bf16[3,64,32,224]{1,0,3,2:T(4,128)(2,1)} %bitcast.58) | data formatting | bytes 5505024 | tf_op jit(solution)/shard_map/all_to_all | solution.py:68
  172.6 1.7 copy-done
  174.3 1.8 fusion.25
  176.1 8.0 %fusion.27 = f32[2048,224]{0,1:T(8,128)} fusion(bf16[2048,2048]{1,0:T(8,128)(2,1)} %fusion.2, bf16[2048,224]{1,0:T(8,128)(2,1)S(1)} %bitcast.68), kind=kOutput, calls=%fused_computation.41 | convolution fusion | flops 1879048192 | bytes 11141120 | tf_op jit(solution)/shard_map/dot_general | solution.py:45
  184.1 4.0 %fusion.28 = f32[2048,224]{0,1:T(8,128)} fusion(bf16[2048,2048]{1,0:T(8,128)(2,1)S(1)} %bitcast.52, bf16[2048,224]{1,0:T(8,128)(2,1)S(1)} %bitcast.67), kind=kOutput, calls=%fused_computation.42 | convolution fusion | flops 1879048192 | bytes 11141120 | tf_op jit(solution)/shard_map/dot_general | solution.py:45
  188.1 4.0 %fusion.29 = f32[2048,224]{0,1:T(8,128)} fusion(bf16[2048,2048]{1,0:T(8,128)(2,1)S(1)} %bitcast.52, bf16[2048,224]{1,0:T(8,128)(2,1)S(1)} %bitcast.66), kind=kOutput, calls=%fused_computation.43 | convolution fusion | flops 1879048192 | bytes 11141120 | tf_op jit(solution)/shard_map/dot_general | solution.py:45
  192.1 15.3 %fusion.7 = f32[2048,2048]{1,0:T(8,128)} fusion(bf16[2048,2048]{1,0:T(8,128)(2,1)} %fusion.2, bf16[2048,224]{1,0:T(8,128)(2,1)} %bitcast.64, f32[2048,224]{0,1:T(8,128)} %fusion.27, bf16[3,224,2048]{2,1,0:T(8,128)(2,1)} %all-gather.8.cloned.1.call-done), kind=kOutput, calls=%fused_computation.13 | convolution fusion | flops 3760848896 | bytes 28966912 | tf_op jit(solution)/shard_map/dot_general | solution.py:48
  207.4 15.5 %fusion.6 = f32[2048,2048]{1,0:T(8,128)} fusion(bf16[2048,2048]{1,0:T(8,128)(2,1)} %fusion.2, bf16[2048,224]{1,0:T(8,128)(2,1)} %bitcast.63, f32[2048,224]{0,1:T(8,128)} %fusion.28, bf16[3,224,2048]{2,1,0:T(8,128)(2,1)} %all-gather.8.cloned.1.call-done), kind=kOutput, calls=%fused_computation.12 | convolution fusion | flops 3760848896 | bytes 28966912 | tf_op jit(solution)/shard_map/dot_general | solution.py:48
  222.9 19.2 %add_convert_fusion = bf16[2048,2048]{1,0:T(8,128)(2,1)} fusion(f32[2048,2048]{1,0:T(8,128)} %fusion.6, f32[2048,2048]{1,0:T(8,128)} %fusion.7, f32[2048]{0:T(1024)S(1)} %bitcast.70, f32[2048]{0:T(1024)S(1)} %bitcast.71, f32[2048]{0:T(1024)S(1)} %bitcast.69, bf16[3,224,2048]{2,1,0:T(8,128)(2,1)} %all-gather.8.cloned.1.call-done, ...), kind=kOutput, calls=%fused_computation.4 | convolution fusion | flops 3786014720 | bytes 54157312 | tf_op jit(solution)/shard_map/dot_general | solution.py:48
  242.0 8.3 %copy.45 = bf16[4,4,2,64,2048]{4,3,2,1,0:T(8,128)(2,1)} copy(bf16[4,4,2,64,2048]{4,3,1,0,2:T(8,128)(2,1)} %bitcast.54) | data formatting | bytes 16777216 | tf_op jit(solution)/shard_map/transpose | solution.py:13
  250.4 80.8 %reduce-scatter.4.cloned.1.call-done = bf16[8,64,2048]{2,1,0:T(8,128)(2,1)} async-done(((bf16[32,64,2048]{2,1,0:T(8,128)(2,1)}), bf16[8,64,2048]{2,1,0:T(8,128)(2,1)}) %reduce-scatter.4.cloned.1.call-update) | async-done | bytes 2097168 | tf_op jit(solution)/shard_map/reduce_scatter | solution.py:16
  331.3 31.6 %reduce-scatter.6.cloned.1.call-done = bf16[2,64,2048]{2,1,0:T(8,128)(2,1)} async-done(((bf16[8,64,2048]{2,1,0:T(8,128)(2,1)}), bf16[2,64,2048]{2,1,0:T(8,128)(2,1)}) %reduce-scatter.6.cloned.1.call-update) | async-done | bytes 524304 | tf_op jit(solution)/shard_map/reduce_scatter | solution.py:16
  362.9 2.7 copy.46
  365.6 4.7 %copy.47 = bf16[3,2048,224]{1,2,0:T(8,128)(2,1)} copy(bf16[3,2048,224]{2,1,0:T(8,128)(2,1)} %bitcast.61) | data formatting | bytes 5505024
  370.3 12.2 %reduce-scatter.8.cloned.1.call-done = bf16[1,64,2048]{2,1,0:T(8,128)(2,1)} async-done(((bf16[2,64,2048]{2,1,0:T(8,128)(2,1)}), bf16[1,64,2048]{2,1,0:T(8,128)(2,1)}) %reduce-scatter.8.cloned.1.call-update) | async-done | bytes 262160 | tf_op jit(solution)/shard_map/reduce_scatter | solution.py:16
  382.5 1.5 copy.49
  (32 shorter events, 1.4 us)
Async XLA Ops:
  7.2 37.4 %all-gather.4.cloned.1.call-start = ((), (), s32[]{:S(2)}) async-start(), calls=%async_computation.5 | async-start | bytes 3440640 | tf_op jit(solution)/shard_map/all_gather | solution.py:62
  10.3 66.4 %all-gather.6.cloned.1.call-start = ((), (), s32[]{:S(2)}) async-start(), calls=%async_computation.6 | async-start | bytes 3440640 | tf_op jit(solution)/shard_map/all_gather | solution.py:63
  67.2 41.4 %all-to-all-start = ((bf16[32,2,21504]{2,1,0:T(2,128)(2,1)}), bf16[32,2,21504]{2,1,0:T(2,128)(2,1)S(1)}, u32[]{:S(2)}, u32[]{:S(2)}) async-start(bf16[32,2,21504]{2,1,0:T(2,128)(2,1)} %reshape.105), calls=%async_computation | async-start | bytes 5505024 | tf_op jit(solution)/shard_map/all_to_all | solution.py:67
  74.3 2.4 copy-start.2
  74.3 117.9 %all-gather.8.cloned.1.call-start = ((), (), s32[]{:S(2)}) async-start(), calls=%async_computation.7 | async-start | bytes 3440640 | tf_op jit(solution)/shard_map/all_gather | solution.py:64
  99.4 15.6 %copy-start.3 = (s32[1,2048,2]{1,2,0:T(2,128)S(1)}, s32[1,2048,2]{1,2,0:T(2,128)}, u32[]{:S(2)}) copy-start(s32[1,2048,2]{1,2,0:T(2,128)} %param.12) | copy-start | bytes 49156
  108.6 39.9 %all-to-all-start.1 = ((bf16[32,2,21504]{2,1,0:T(2,128)(2,1)}), bf16[32,2,21504]{2,1,0:T(2,128)(2,1)}, u32[]{:S(2)}, u32[]{:S(2)}) async-start(bf16[32,2,21504]{2,1,0:T(2,128)(2,1)} %reshape.107), calls=%async_computation.1 | async-start | bytes 5505024 | tf_op jit(solution)/shard_map/all_to_all | solution.py:68
  115.0 216.3 %reduce-scatter.4.cloned.1.call-start = ((), (), s32[]{:S(2)}) async-start(), calls=%async_computation.8 | async-start | bytes 10485760 | tf_op jit(solution)/shard_map/reduce_scatter | solution.py:16
  172.4 1.9 copy-start
  174.3 9.8 %slice-start = ((s8[8388608]{0:T(1024)(128)(4,1)}), s8[4194304]{0:T(1024)(128)(4,1)S(1)}, s32[]{:S(2)}) async-start(s8[8388608]{0:T(1024)(128)(4,1)} %bitcast.51), calls=%async_computation.11 | async-start | bytes 8388608
  176.1 8.0 %slice-start.1 = ((s8[8388608]{0:T(1024)(128)(4,1)}), s8[4194304]{0:T(1024)(128)(4,1)S(1)}, s32[]{:S(2)}) async-start(s8[8388608]{0:T(1024)(128)(4,1)} %bitcast.51), calls=%async_computation.12 | async-start | bytes 8388608
  250.3 112.5 %reduce-scatter.6.cloned.1.call-start = ((), (), s32[]{:S(2)}) async-start(), calls=%async_computation.9 | async-start | bytes 2621440 | tf_op jit(solution)/shard_map/reduce_scatter | solution.py:16
  331.2 51.3 %reduce-scatter.8.cloned.1.call-start = ((), (), s32[]{:S(2)}) async-start(), calls=%async_computation.10 | async-start | bytes 786432 | tf_op jit(solution)/shard_map/reduce_scatter | solution.py:16
  365.6 16.9 %copy-start.1 = (bf16[3,224,2048]{2,1,0:T(8,128)(2,1)S(1)}, bf16[3,224,2048]{2,1,0:T(8,128)(2,1)}, u32[]{:S(2)}) copy-start(bf16[3,224,2048]{2,1,0:T(8,128)(2,1)} %all-gather.8.cloned.1.call-done) | copy-start | bytes 8257540
Sparse Core Ops, SparseCore 0:
  10.4 34.0 all-gather.3
  46.8 29.6 all-gather.5
  78.1 74.4 all-gather.7
  250.5 80.7 reduce-scatter.3
  333.5 29.3 reduce-scatter.5
  365.6 16.8 reduce-scatter.7
where the time goes:
time: 393 us; the launch traced here: 391 us
  waiting for transfers between devices  169 us (43%)
  local copies, waits for them, and re-layouts  110 us (28%)
  matrix products  65.9 us (17%)
  other arithmetic  18.6 us (5%)
  between operations  14.2 us (4%)
  starting transfers between devices  13.6 us (3%)
    reduce_scatter x3, waiting for transfers between devices, reduced_to_own(): blocks = lax.psum_scatter(blocks, axes[k], scatter_dimension=0, tiled=True)  125 us
    unnamed x19, local copies, waits for them, and re-layouts  57 us
    dot_general x3, matrix products, expert_term(): projected = jnp.dot(hidden, down_weight, preferred_element_type=jnp.float32)  49.9 us
    all_gather x1, waiting for transfers between devices, shards(): lax.all_gather(gate_local, ('gr', 'tp'), axis=2, tiled=True)  33.5 us
    dot_general x3, matrix products, expert_term(): gate_act = jnp.dot(normed, gate_weight, preferred_element_type=jnp.float32)  16 us
    all_to_all x1, local copies, waits for them, and re-layouts, shards(): lax.all_to_all(up_rows, FS, split_axis=2, concat_axis=1, tiled=True)  11.4 us
    all_to_all x1, local copies, waits for them, and re-layouts, shards(): lax.all_to_all(gate_rows, FS, split_axis=2, concat_axis=1, tiled=True)  10.7 us
    all_gather x1, local copies, waits for them, and re-layouts, shards(): lax.all_gather(up_local, ('gr', 'tp'), axis=2, tiled=True)  10.1 us
  transfers between devices with their start and end apart: 8, of which 6 were waited for; matrix products, arithmetic and copies ran while one was open for 33% of the time, Pallas kernels for 0%

commit v1 on v0

--- a/solution.py
+++ b/solution.py
@@ -1,3 +1,4 @@
+import functools
 import jax
 import jax.numpy as jnp
 from jax import lax
@@ -5,6 +6,14 @@
 from jax.sharding import PartitionSpec as P
 
 FS = ("fs_0", "fs_1", "fs_2")
+
+
+def apply_the_pieces_all(original, along_axis):
+    val2 = jax.lax.all_gather(original, axis_name=along_axis)
+    return jnp.concatenate(val2, 2)
+
+
+plan_chains_on = functools.partial(apply_the_pieces_all, along_axis=("gr", "tp"))
 
 
 def reduced_to_own(blocks, axes, order):
@@ -59,7 +68,7 @@
     combine = mixing(route[0], route_weight[0], experts)
     width = normed.shape[1]
     gate_rows, up_rows, down_out = (
-        lax.all_gather(gate_local, ("gr", "tp"), axis=2, tiled=True),
+        plan_chains_on(gate_local),
         lax.all_gather(up_local, ("gr", "tp"), axis=2, tiled=True),
         lax.all_gather(down_local, ("gr", "tp"), axis=2, tiled=True),
     )

time: 393 us -> 395 us (level)
  local copies, waits for them, and re-layouts: 110 us -> 123 us
  waiting for transfers between devices: 169 us -> 156 us
    reduce_scatter x3, waiting for transfers between devices: 125 us -> 113 us  [reduced_to_own(): blocks = lax.psum_scatter(blocks, axes[k], scatter_dimension=0, tiled=True)]
    reshape x0 -> x1, local copies, waits for them, and re-layouts: none -> 10.1 us  [apply_the_pieces_all(): return jnp.concatenate(val2, 2)]
    all_gather x1 -> x0, local copies, waits for them, and re-layouts: 10.1 us -> none  [shards(): lax.all_gather(gate_local, ('gr', 'tp'), axis=2, tiled=True)]
    all_to_all x1 -> x2, local copies, waits for them, and re-layouts: 10.7 us -> 19.4 us  [shards(): lax.all_to_all(gate_rows, FS, split_axis=2, concat_axis=1, tiled=True)]
    slice x1 -> x4, local copies, waits for them, and re-layouts: 0.22 us -> 5 us  [shards(): gate_out[index]]
    unnamed x19 -> x21, local copies, waits for them, and re-layouts: 57 us -> 57.4 us
  transfers between devices with their start and end apart: 8 -> 8, of which waited for: 6 -> 5; matrix products, arithmetic and copies ran while one was open for 33% -> 36% of each run, Pallas kernels for 0% -> 0%
where the time goes in v1:
time: 395 us; the launch traced here: 392 us
  waiting for transfers between devices  156 us (39%)
  local copies, waits for them, and re-layouts  123 us (31%)
  matrix products  66.3 us (17%)
  other arithmetic  18.7 us (5%)
  between operations  14.3 us (4%)
  starting transfers between devices  13.9 us (4%)
    reduce_scatter x3, waiting for transfers between devices, reduced_to_own(): blocks = lax.psum_scatter(blocks, axes[k], scatter_dimension=0, tiled=True)  113 us
    unnamed x21, local copies, waits for them, and re-layouts  57.4 us
    dot_general x3, matrix products, expert_term(): projected = jnp.dot(hidden, down_weight, preferred_element_type=jnp.float32)  50 us
    all_gather x1, waiting for transfers between devices, apply_the_pieces_all(): val2 = jax.lax.all_gather(original, axis_name=along_axis)  33.5 us
    all_to_all x2, local copies, waits for them, and re-layouts, shards(): lax.all_to_all(gate_rows, FS, split_axis=2, concat_axis=1, tiled=True)  19.4 us
    dot_general x3, matrix products, expert_term(): gate_act = jnp.dot(normed, gate_weight, preferred_element_type=jnp.float32)  16.3 us
    all_to_all x1, local copies, waits for them, and re-layouts, shards(): lax.all_to_all(up_rows, FS, split_axis=2, concat_axis=1, tiled=True)  10.9 us
    reshape x1, local copies, waits for them, and re-layouts, apply_the_pieces_all(): return jnp.concatenate(val2, 2)  10.1 us
  transfers between devices with their start and end apart: 8, of which 5 were waited for; matrix products, arithmetic and copies ran while one was open for 36% of the time, Pallas kernels for 0%

profile of v1, /device:TPU:1, one launch (start us, length us, event | category | flops | bytes accessed | tf_op | source)
XLA Modules:
  0.0 392.5 jit_solution(5460865667643021811)
XLA Ops:
  7.2 3.1 multiply_convert_fusion
  11.1 33.5 %all-gather.9.cloned.1.call-done = bf16[12,64,1792]{2,1,0:T(8,128)(2,1)} async-done(((bf16[3,64,1792]{2,1,0:T(8,128)(2,1)}), bf16[12,64,1792]{2,1,0:T(8,128)(2,1)}) %all-gather.9.cloned.1.call-update) | async-done | bytes 2752528 | tf_op jit(solution)/shard_map/all_gather | solution.py:12
  44.5 10.1 %copy.55 = bf16[4,3,64,1792]{2,1,3,0:T(4,128)(2,1)} copy(bf16[4,3,64,1792]{3,2,1,0:T(8,128)(2,1)} %bitcast.73) | data formatting | bytes 5505024 | tf_op jit(solution)/shard_map/reshape | solution.py:13
  54.7 12.7 %reshape.114 = bf16[32,2,21504]{2,1,0:T(2,128)(2,1)} reshape(bf16[7168,3,64]{2,1,0:T(4,128)(2,1)} %bitcast.63) | data formatting | bytes 5505024
  67.4 6.9 %all-to-all-start = ((bf16[32,2,21504]{2,1,0:T(2,128)(2,1)}), bf16[32,2,21504]{2,1,0:T(2,128)(2,1)S(1)}, u32[]{:S(2)}, u32[]{:S(2)}) async-start(bf16[32,2,21504]{2,1,0:T(2,128)(2,1)} %reshape.114), calls=%async_computation | async-start | bytes 5505024 | tf_op jit(solution)/shard_map/all_to_all | solution.py:76
  74.4 2.3 convert_element_type.47
  76.9 10.1 %copy.44 = bf16[3,64,7168]{1,0,2:T(4,128)(2,1)} copy(bf16[3,64,7168]{2,1,0:T(8,128)(2,1)} %all-gather.5.cloned.1.call-done) | data formatting | bytes 5505024 | tf_op jit(solution)/shard_map/all_gather | solution.py:72
  87.0 12.6 %reshape.116 = bf16[32,2,21504]{2,1,0:T(2,128)(2,1)} reshape(bf16[7168,3,64]{2,1,0:T(4,128)(2,1)} %bitcast.64) | data formatting | bytes 5505024
  99.6 8.8 %all-to-all-done = bf16[32,2,21504]{2,1,0:T(2,128)(2,1)S(1)} async-done(((bf16[32,2,21504]{2,1,0:T(2,128)(2,1)}), bf16[32,2,21504]{2,1,0:T(2,128)(2,1)S(1)}, u32[]{:S(2)}, u32[]{:S(2)}) %all-to-all-start) | async-done | bytes 2752544 | tf_op jit(solution)/shard_map/all_to_all | solution.py:76
  108.4 6.8 %all-to-all-start.1 = ((bf16[32,2,21504]{2,1,0:T(2,128)(2,1)}), bf16[32,2,21504]{2,1,0:T(2,128)(2,1)}, u32[]{:S(2)}, u32[]{:S(2)}) async-start(bf16[32,2,21504]{2,1,0:T(2,128)(2,1)} %reshape.116), calls=%async_computation.1 | async-start | bytes 5505024 | tf_op jit(solution)/shard_map/all_to_all | solution.py:77
  115.3 5.1 %fusion = f32[2048]{0:T(1024)S(1)} fusion(bf16[1,2048,2048]{2,1,0:T(8,128)(2,1)} %param.7), kind=kLoop, calls=%fused_computation.2 | loop fusion | flops 12580864 | bytes 8396800 | tf_op jit(solution)/shard_map/reduce_sum | solution.py:42
  120.4 8.0 %fusion.2 = bf16[2048,2048]{1,0:T(8,128)(2,1)} fusion(bf16[1,2048,2048]{2,1,0:T(8,128)(2,1)} %param.7, f32[2048]{0:T(1024)S(1)} %add_rsqrt_fusion), kind=kLoop, calls=%fused_computation.5 | loop fusion | flops 12582912 | bytes 16785408 | tf_op jit(solution)/shard_map/convert_element_type | solution.py:43
  128.4 8.6 %reshape.115 = bf16[7168,3,64]{2,1,0:T(4,128)(2,1)} reshape(bf16[32,2,21504]{2,1,0:T(2,128)(2,1)S(1)} %all-to-all-done) | data formatting | bytes 5505024
  137.1 8.1 %copy.53 = bf16[3,64,32,224]{3,2,1,0:T(8,128)(2,1)S(1)} copy(bf16[3,64,32,224]{1,0,3,2:T(4,128)(2,1)} %bitcast.59) | data formatting | bytes 5505024 | tf_op jit(solution)/shard_map/all_to_all | solution.py:76
  145.4 1.6 copy.48
  148.5 1.6 copy.46
  150.1 12.4 %reshape.117 = bf16[7168,3,64]{2,1,0:T(4,128)(2,1)} reshape(bf16[32,2,21504]{2,1,0:T(2,128)(2,1)} %all-to-all-done.1) | data formatting | bytes 5505024
  162.6 10.9 %copy.45 = bf16[3,64,32,224]{3,1,2,0:T(8,128)(2,1)S(1)} copy(bf16[3,64,32,224]{1,0,3,2:T(4,128)(2,1)} %bitcast.65) | data formatting | bytes 5505024 | tf_op jit(solution)/shard_map/all_to_all | solution.py:77
  173.5 1.8 fusion.25
  175.3 8.2 %fusion.29 = f32[2048,224]{0,1:T(8,128)} fusion(bf16[2048,2048]{1,0:T(8,128)(2,1)} %fusion.2, bf16[2048,224]{1,0:T(8,128)(2,1)S(1)} %bitcast.74), kind=kOutput, calls=%fused_computation.43 | convolution fusion | flops 1879048192 | bytes 11141120 | tf_op jit(solution)/shard_map/dot_general | solution.py:54
  183.5 4.0 %fusion.28 = f32[2048,224]{0,1:T(8,128)} fusion(bf16[2048,2048]{1,0:T(8,128)(2,1)S(1)} %bitcast.58, bf16[2048,224]{1,0:T(8,128)(2,1)S(1)} %bitcast.75), kind=kOutput, calls=%fused_computation.42 | convolution fusion | flops 1879048192 | bytes 11141120 | tf_op jit(solution)/shard_map/dot_general | solution.py:54
  187.6 4.0 %fusion.27 = f32[2048,224]{0,1:T(8,128)} fusion(bf16[2048,2048]{1,0:T(8,128)(2,1)S(1)} %bitcast.58, bf16[2048,224]{1,0:T(8,128)(2,1)S(1)} %bitcast.76), kind=kOutput, calls=%fused_computation.41 | convolution fusion | flops 1879048192 | bytes 11141120 | tf_op jit(solution)/shard_map/dot_general | solution.py:54
  191.6 15.3 %fusion.7 = f32[2048,2048]{1,0:T(8,128)} fusion(bf16[2048,2048]{1,0:T(8,128)(2,1)} %fusion.2, bf16[2048,224]{1,0:T(8,128)(2,1)} %bitcast.71, f32[2048,224]{0,1:T(8,128)} %fusion.27, bf16[3,224,2048]{2,1,0:T(8,128)(2,1)} %all-gather.7.cloned.1.call-done), kind=kOutput, calls=%fused_computation.13 | convolution fusion | flops 3760848896 | bytes 28966912 | tf_op jit(solution)/shard_map/dot_general | solution.py:57
  206.9 15.5 %fusion.6 = f32[2048,2048]{1,0:T(8,128)} fusion(bf16[2048,2048]{1,0:T(8,128)(2,1)} %fusion.2, bf16[2048,224]{1,0:T(8,128)(2,1)} %bitcast.70, f32[2048,224]{0,1:T(8,128)} %fusion.28, bf16[3,224,2048]{2,1,0:T(8,128)(2,1)} %all-gather.7.cloned.1.call-done), kind=kOutput, calls=%fused_computation.12 | convolution fusion | flops 3760848896 | bytes 28966912 | tf_op jit(solution)/shard_map/dot_general | solution.py:57
  222.3 19.3 %add_convert_fusion = bf16[2048,2048]{1,0:T(8,128)(2,1)} fusion(f32[2048,2048]{1,0:T(8,128)} %fusion.6, f32[2048,2048]{1,0:T(8,128)} %fusion.7, f32[2048]{0:T(1024)S(1)} %bitcast.78, f32[2048]{0:T(1024)S(1)} %bitcast.79, f32[2048]{0:T(1024)S(1)} %bitcast.77, bf16[3,224,2048]{2,1,0:T(8,128)(2,1)} %all-gather.7.cloned.1.call-done, ...), kind=kOutput, calls=%fused_computation.4 | convolution fusion | flops 3786014720 | bytes 54157312 | tf_op jit(solution)/shard_map/dot_general | solution.py:57
  241.6 8.3 %copy.49 = bf16[4,4,2,64,2048]{4,3,2,1,0:T(8,128)(2,1)} copy(bf16[4,4,2,64,2048]{4,3,1,0,2:T(8,128)(2,1)} %bitcast.62) | data formatting | bytes 16777216 | tf_op jit(solution)/shard_map/transpose | solution.py:22
  249.9 80.7 %reduce-scatter.4.cloned.1.call-done = bf16[8,64,2048]{2,1,0:T(8,128)(2,1)} async-done(((bf16[32,64,2048]{2,1,0:T(8,128)(2,1)}), bf16[8,64,2048]{2,1,0:T(8,128)(2,1)}) %reduce-scatter.4.cloned.1.call-update) | async-done | bytes 2097168 | tf_op jit(solution)/shard_map/reduce_scatter | solution.py:25
  330.7 31.6 %reduce-scatter.6.cloned.1.call-done = bf16[2,64,2048]{2,1,0:T(8,128)(2,1)} async-done(((bf16[8,64,2048]{2,1,0:T(8,128)(2,1)}), bf16[2,64,2048]{2,1,0:T(8,128)(2,1)}) %reduce-scatter.6.cloned.1.call-update) | async-done | bytes 524304 | tf_op jit(solution)/shard_map/reduce_scatter | solution.py:25
  362.3 11.4 %copy.54 = bf16[3,64,32,224]{3,1,2,0:T(8,128)(2,1)} copy(bf16[3,64,32,224]{1,0,3,2:T(4,128)(2,1)} %bitcast.60) | data formatting | bytes 5505024 | tf_op jit(solution)/shard_map/all_to_all | solution.py:76
  373.7 4.6 %copy.50 = bf16[3,2048,224]{1,2,0:T(8,128)(2,1)} copy(bf16[3,2048,224]{2,1,0:T(8,128)(2,1)} %bitcast.69) | data formatting | bytes 5505024
  378.3 2.7 copy.51
  382.0 3.7 copy.57
  (38 shorter events, 4.1 us)
Async XLA Ops:
  7.2 37.4 %all-gather.9.cloned.1.call-start = ((), (), s32[]{:S(2)}) async-start(), calls=%async_computation.10 | async-start | bytes 3440640 | tf_op jit(solution)/shard_map/all_gather | solution.py:12
  10.3 66.6 %all-gather.5.cloned.1.call-start = ((), (), s32[]{:S(2)}) async-start(), calls=%async_computation.5 | async-start | bytes 3440640 | tf_op jit(solution)/shard_map/all_gather | solution.py:72
  67.4 41.0 %all-to-all-start = ((bf16[32,2,21504]{2,1,0:T(2,128)(2,1)}), bf16[32,2,21504]{2,1,0:T(2,128)(2,1)S(1)}, u32[]{:S(2)}, u32[]{:S(2)}) async-start(bf16[32,2,21504]{2,1,0:T(2,128)(2,1)} %reshape.114), calls=%async_computation | async-start | bytes 5505024 | tf_op jit(solution)/shard_map/all_to_all | solution.py:76
  74.3 2.4 copy-start.3
  74.3 2.5 copy-start.4
  74.3 117.3 %all-gather.7.cloned.1.call-start = ((), (), s32[]{:S(2)}) async-start(), calls=%async_computation.6 | async-start | bytes 3440640 | tf_op jit(solution)/shard_map/all_gather | solution.py:73
  108.4 41.8 %all-to-all-start.1 = ((bf16[32,2,21504]{2,1,0:T(2,128)(2,1)}), bf16[32,2,21504]{2,1,0:T(2,128)(2,1)}, u32[]{:S(2)}, u32[]{:S(2)}) async-start(bf16[32,2,21504]{2,1,0:T(2,128)(2,1)} %reshape.116), calls=%async_computation.1 | async-start | bytes 5505024 | tf_op jit(solution)/shard_map/all_to_all | solution.py:77
  115.2 215.5 %reduce-scatter.4.cloned.1.call-start = ((), (), s32[]{:S(2)}) async-start(), calls=%async_computation.7 | async-start | bytes 10485760 | tf_op jit(solution)/shard_map/reduce_scatter | solution.py:25
  173.5 1.8 copy-start
  173.5 10.0 %slice-start = ((s8[8388608]{0:T(1024)(128)(4,1)}), s8[4194304]{0:T(1024)(128)(4,1)S(1)}, s32[]{:S(2)}) async-start(s8[8388608]{0:T(1024)(128)(4,1)} %bitcast.57), calls=%async_computation.11 | async-start | bytes 8388608
  175.3 8.2 %slice-start.1 = ((s8[8388608]{0:T(1024)(128)(4,1)}), s8[4194304]{0:T(1024)(128)(4,1)S(1)}, s32[]{:S(2)}) async-start(s8[8388608]{0:T(1024)(128)(4,1)} %bitcast.57), calls=%async_computation.12 | async-start | bytes 8388608
  175.3 8.2 %copy-start.1 = (bf16[1,32,64,224]{3,2,1,0:T(8,128)(2,1)S(1)}, bf16[1,32,64,224]{3,2,1,0:T(8,128)(2,1)}, u32[]{:S(2)}) copy-start(bf16[1,32,64,224]{3,2,1,0:T(8,128)(2,1)} %copy.47) | copy-start | bytes 2752516
  183.5 4.0 %copy-start.2 = (bf16[1,32,64,224]{3,2,1,0:T(8,128)(2,1)S(1)}, bf16[1,32,64,224]{3,2,1,0:T(8,128)(2,1)}, u32[]{:S(2)}) copy-start(bf16[1,32,64,224]{3,2,1,0:T(8,128)(2,1)} %copy.46) | copy-start | bytes 2752516
  249.9 112.4 %reduce-scatter.6.cloned.1.call-start = ((), (), s32[]{:S(2)}) async-start(), calls=%async_computation.8 | async-start | bytes 2621440 | tf_op jit(solution)/shard_map/reduce_scatter | solution.py:25
  330.7 51.3 %reduce-scatter.8.cloned.1.call-start = ((), (), s32[]{:S(2)}) async-start(), calls=%async_computation.9 | async-start | bytes 786432 | tf_op jit(solution)/shard_map/reduce_scatter | solution.py:25
Sparse Core Ops, SparseCore 0:
  10.4 34.0 all-gather.8
  46.8 29.6 all-gather.4
  78.1 74.5 all-gather.6
  250.0 80.5 reduce-scatter.3
  332.9 29.3 reduce-scatter.5
  365.1 16.8 reduce-scatter.7
